TPU v7x, 32 devices: a whole 2x2x4 slice. The times are simulated.
32 devices in a mesh: sp: 8 (over z, x), tp: 4 (over y, core).
Axes of the slice: x: 2, y: 2, z: 4, core: 2. Of those that a mesh axis runs over, the one named last changes fastest.
Arguments:
- residual: bfloat16 [2048, 2048], P('sp', 'tp'), may hold values from -26 to 26
- queries: bfloat16 [2048, 2048], P('tp', 'sp'), may hold values from -6 to 6
- keys: bfloat16 [2048, 2048], P('tp', 'sp'), may hold values from -6 to 6
- values: bfloat16 [2048, 2048], P('tp', 'sp'), may hold values from -12 to 12
- forget_cache: float32 [32, 2048], P('tp', 'sp'), as said below
- out_weight: bfloat16 [2048, 2048], P('tp'), may hold values from -0.125 to 0.125
- norm_gain: float32 [2048], replicated, may hold values from 0.1 to 1.9
- routes: int32 [2048, 2], P('sp'), may hold values from 0 to 7, all different within a row; in each aligned block of 256 rows (0 to 255, 256 to 511, ...) at most 80 rows name the same one
- route_weight: float32 [2048, 2], P('sp'), may hold values from 0.2 to 1
- gate_weight: bfloat16 [8, 2048, 4096], P('sp', None, 'tp'), may hold values from -0.125 to 0.125
- up_weight: bfloat16 [8, 2048, 4096], P('sp', None, 'tp'), may hold values from -0.125 to 0.125
- down_weight: bfloat16 [8, 4096, 2048], P('sp', 'tp'), may hold values from -0.09375 to 0.09375
Outputs:
- updated: bfloat16 [2048, 2048], P('sp', 'tp')
Inputs may be any that keep to these rules, and one draw needn't show every extreme that they name: `routes`: each row names 2 different experts; within the 256 rows of one index of sp no expert is named by more than 80 rows, and in the rows of some index some expert is named by exactly 80. `forget_cache`: each head's row never rises from one position to the next.
All inputs are finite; a program needn't handle non-finite values.
Results may differ from a plain program's by a relative error of at most 0.013.
Values may be sent and summed in bfloat16 or wider, within the bound.
A program may use at most 64 MiB of HBM per device.

v0:
```python
import jax
import jax.numpy as jnp
from jax import lax
from jax.sharding import PartitionSpec as P

norm_eps = 1e-06
masked_score = -1e30
key_span = 1024


def shards(
    residual,
    queries,
    keys,
    values,
    forget_cache,
    out_weight,
    norm_gain,
    routes,
    route_weight,
    gate_weight,
    up_weight,
    down_weight,
):
    sp_count = lax.axis_size("sp")
    token_count, local_width = residual.shape
    model_width = norm_gain.shape[0]
    head_count = forget_cache.shape[0]
    head_width = queries.shape[0] // head_count
    first_token = lax.axis_index("sp") * token_count
    last_token = first_token + token_count - 1
    query_heads = queries.reshape(head_count, head_width, token_count)
    query_place = first_token + jnp.arange(token_count, dtype=jnp.int32)
    score_scale = head_width ** (-0.5)

    def attend_block(state_now, key_block, value_block, cache_block, key_first):
        running_peak, running_total, running_sum = state_now
        block_length = key_block.shape[1]
        key_heads = key_block.reshape(head_count, head_width, block_length)
        value_heads = value_block.reshape(head_count, head_width, block_length)
        scores = (
            jnp.einsum("hdq,hdk->hqk", query_heads, key_heads, preferred_element_type=jnp.float32)
            * score_scale
        )
        scores = scores + forget_cache[:, :, None] - cache_block[:, None, :]
        key_place = key_first + jnp.arange(block_length, dtype=jnp.int32)
        allowed = key_place[None, :] <= query_place[:, None]
        scores = jnp.where(allowed[None], scores, masked_score)
        new_peak = jnp.maximum(running_peak, jnp.max(scores, axis=2))
        weights = jnp.exp(scores - new_peak[:, :, None])
        shrink = jnp.exp(running_peak - new_peak)
        new_total = running_total * shrink + jnp.sum(weights, axis=2)
        new_sum = running_sum * shrink[:, None, :] + jnp.einsum(
            "hdk,hqk->hdq",
            value_heads,
            weights.astype(jnp.bfloat16),
            preferred_element_type=jnp.float32,
        )
        return (new_peak, new_total, new_sum)

    initial = (
        jnp.full((head_count, token_count), masked_score, jnp.float32),
        jnp.zeros((head_count, token_count), jnp.float32),
        jnp.zeros((head_count, head_width, token_count), jnp.float32),
    )
    key_part = lax.all_gather(keys.astype(jnp.float32), "sp", axis=1, tiled=True).astype(
        jnp.bfloat16
    )
    value_part = lax.all_gather(values.astype(jnp.float32), "sp", axis=1, tiled=True).astype(
        jnp.bfloat16
    )
    cache_part = lax.all_gather(forget_cache, "sp", axis=1, tiled=True)
    part_length = key_part.shape[1]
    block_length = key_span

    def one_block(block_index, state_in):
        start_column = block_index * block_length
        key_block = lax.dynamic_slice_in_dim(key_part, start_column, block_length, 1)
        value_block = lax.dynamic_slice_in_dim(value_part, start_column, block_length, 1)
        cache_block = lax.dynamic_slice_in_dim(cache_part, start_column, block_length, 1)
        return lax.cond(
            start_column <= last_token,
            lambda inner: attend_block(inner, key_block, value_block, cache_block, start_column),
            lambda inner: inner,
            state_in,
        )

    final_peak, final_total, final_sum = lax.fori_loop(
        0, part_length // block_length, one_block, initial
    )
    attended = (
        (final_sum / final_total[:, None, :])
        .astype(jnp.bfloat16)
        .reshape(head_count * head_width, token_count)
    )
    projected = lax.dot_general(
        attended, out_weight, (((0,), (0,)), ((), ())), preferred_element_type=jnp.float32
    )
    head_sum = lax.psum_scatter(
        projected.astype(jnp.bfloat16), "tp", scatter_dimension=1, tiled=True
    ).astype(jnp.float32)
    stream = (residual.astype(jnp.float32) + head_sum).astype(jnp.bfloat16)
    top_count = routes.shape[1]
    item_count = token_count * top_count
    capacity = max(2, token_count * top_count * 5 // (4 * sp_count))
    expert_of = routes.reshape(item_count)
    onehot = (expert_of[:, None] == jnp.arange(sp_count, dtype=jnp.int32)[None, :]).astype(
        jnp.int32
    )
    earlier = jnp.cumsum(onehot, axis=0) - onehot
    target = expert_of * capacity + jnp.sum(earlier * onehot, axis=1)
    matches = target[None, :] == jnp.arange(sp_count * capacity, dtype=jnp.int32)[:, None]
    filled = jnp.any(matches, axis=1)
    source_row = (
        jnp.sum(jnp.where(matches, jnp.arange(item_count, dtype=jnp.int32)[None, :], 0), axis=1)
        // top_count
    )
    local_rows = stream.astype(jnp.float32)
    squares = lax.psum(jnp.sum(local_rows * local_rows, axis=1), "tp")
    row_scale = lax.rsqrt(squares / model_width + norm_eps)
    local_gain = lax.dynamic_slice_in_dim(
        norm_gain, lax.axis_index("tp") * local_width, local_width
    )
    normed = (local_rows * row_scale[:, None] * local_gain[None, :]).astype(jnp.bfloat16)
    taken_rows = jnp.take(normed, source_row, axis=0)
    taken_rows = jnp.where(filled[:, None], taken_rows, jnp.zeros((), normed.dtype))
    arrived = lax.all_gather(
        lax.all_to_all(
            taken_rows.reshape(sp_count, capacity, normed.shape[1]),
            "sp",
            split_axis=0,
            concat_axis=0,
            tiled=True,
        ),
        "tp",
        axis=2,
        tiled=True,
    )
    source_count = arrived.shape[0]
    slot_count = arrived.shape[1]
    flat_rows = arrived.reshape(source_count * slot_count, model_width)
    gate_value = jnp.dot(flat_rows, gate_weight[0], preferred_element_type=jnp.float32)
    up_value = jnp.dot(flat_rows, up_weight[0], preferred_element_type=jnp.float32)
    hidden = (jax.nn.silu(gate_value) * up_value).astype(jnp.bfloat16)
    down_value = jnp.dot(hidden, down_weight[0], preferred_element_type=jnp.float32)
    summed = lax.psum_scatter(
        down_value.reshape(source_count, slot_count, model_width).astype(jnp.bfloat16),
        "tp",
        scatter_dimension=2,
        tiled=True,
    )
    expert_back = lax.all_to_all(summed, "sp", split_axis=0, concat_axis=0, tiled=True)
    back_rows = expert_back.reshape(sp_count * capacity, local_width)
    picked = (
        jnp.take(back_rows, target, axis=0).astype(jnp.float32)
        * route_weight.reshape(item_count)[:, None]
    )
    mixture = jnp.sum(picked.reshape(token_count, top_count, local_width), axis=1)
    return (stream.astype(jnp.float32) + mixture).astype(jnp.bfloat16)


def solution(mesh):
    return jax.shard_map(
        shards,
        mesh=mesh,
        in_specs=(
            P("sp", "tp"),
            P("tp", "sp"),
            P("tp", "sp"),
            P("tp", "sp"),
            P("tp", "sp"),
            P("tp", None),
            P(),
            P("sp", None),
            P("sp", None),
            P("sp", None, "tp"),
            P("sp", None, "tp"),
            P("sp", "tp", None),
        ),
        out_specs=P("sp", "tp"),
        check_vma=False,
    )
```

profile of v0, /device:TPU:0, one launch (start us, length us, event | category | flops | bytes accessed | tf_op | source)
XLA Modules:
  0.0 300.9 jit_solution(3631287278976109090)
XLA Ops:
  8.1 32.8 %all_gather.13 = f32[8,2048]{1,0:T(8,128)S(1)} all-gather(f32[8,256]{1,0:T(8,128)} %param.20), channel_id=1, replica_groups=mesh['sp'=8,'tp'=4] {'sp'}, dimensions={1}, use_global_device_ids=true | all-gather | bytes 73728 | tf_op jit(solution)/shard_map/all_gather | solution.py:72
  40.9 21.9 %all-gather.4.cloned.1.call-done = bf16[512,2048]{1,0:T(8,128)(2,1)} async-done(((bf16[512,256]{1,0:T(8,128)(2,1)}), bf16[512,2048]{1,0:T(8,128)(2,1)}) %all-gather.4.cloned.1.call-update) | async-done | bytes 2097168 | tf_op jit(solution)/shard_map/all_gather | solution.py:66
  62.8 50.6 %all-gather.6.cloned.1.call-done = bf16[512,2048]{1,0:T(8,128)(2,1)} async-done(((bf16[512,256]{1,0:T(8,128)(2,1)}), bf16[512,2048]{1,0:T(8,128)(2,1)}) %all-gather.6.cloned.1.call-update) | async-done | bytes 2097168 | tf_op jit(solution)/shard_map/all_gather | solution.py:69
  113.5 10.7 %while.18 = (s32[]{:T(128)}, f32[8,256]{1,0:T(8,128)S(1)}, f32[8,256]{1,0:T(8,128)S(1)}, f32[8,64,256]{2,1,0:T(8,128)S(1)}, s32[]{:T(128)}, /*index=5*/bf16[512,...) while((s32[]{:T(128)}, f32[8,256]{1,0:T(8,128)S(1)}, ...), condition=%wide.region_5.6_spmd.clone, body=%wide.region_0.5_spmd.clone.sunk | while | flops 573052160 | bytes 35230096 | solution.py:88
  113.5 10.6 %conditional.3 = ((f32[8,256]{1,0:T(8,128)S(1)}, f32[8,256]{1,0:T(8,128)S(1)}, f32[8,64,256]{2,1,0:T(8,128)S(1)})) conditional(s32[]{:T(128)} %convert_element_type.131, (f32[8,256]{1,0:T(8,128)S(1)}, f32[8,256]{1,0:T(8,128)S(1)}, f32[8,64,256]{2,1,0:T(8,128)S(1)}) %tuple.54, (s32[]{:T(128)}, s32[]{:T(128)}, bf16[512,2048]{1,0:T(8,128)(2,1)}, ...), branch_computations={%region_1.0_spmd, %region_2.4_spmd} | conditional | flops 573052160 | bytes 35228808 | solution.py:81
  113.6 1.8 constant_dynamic-slice_fusion
  115.6 2.9 fusion.4
  118.5 2.7 fusion.3
  121.3 2.8 fusion.8
  124.3 1.7 convolution_convert_fusion
  129.5 30.3 %reduce-scatter.3.cloned.1.call-done = bf16[256,512]{1,0:T(8,128)(2,1)} async-done(((bf16[256,2048]{1,0:T(8,128)(2,1)}), bf16[256,512]{1,0:T(8,128)(2,1)}) %reduce-scatter.3.cloned.1.call-update) | async-done | bytes 262160 | tf_op jit(solution)/shard_map/reduce_scatter | solution.py:99
  160.9 5.8 %psum.7 = f32[256]{0:T(256)S(1)} all-reduce(f32[256]{0:T(256)S(1)} %fusion.25), channel_id=1, replica_groups=mesh['sp'=8,'tp'=4] {'tp'}, use_global_device_ids=true, to_apply=%region_13.14 | all-reduce | flops 256 | bytes 2048 | tf_op jit(solution)/shard_map/psum | solution.py:119
  167.7 2.8 gather_fusion
  170.8 23.1 %all_to_all.10 = bf16[8,80,512]{2,1,0:T(8,128)(2,1)} all-to-all(bf16[8,80,512]{2,1,0:T(8,128)(2,1)S(1)} %select_select_fusion), channel_id=1, replica_groups=mesh['sp'=8,'tp'=4] {'sp'}, dimensions={0} | all-to-all | bytes 1310720 | tf_op jit(solution)/shard_map/all_to_all | solution.py:128
  194.1 23.2 %all-gather.8.cloned.1.call-done = bf16[8,80,2048]{2,1,0:T(8,128)(2,1)} async-done(((bf16[8,80,512]{2,1,0:T(8,128)(2,1)}), bf16[8,80,2048]{2,1,0:T(8,128)(2,1)}) %all-gather.8.cloned.1.call-update) | async-done | bytes 2621456 | tf_op jit(solution)/shard_map/all_gather | solution.py:127
  217.3 5.6 %fusion.15 = f32[640,1024]{1,0:T(8,128)S(1)} fusion(bf16[640,2048]{1,0:T(8,128)(2,1)} %bitcast.58, bf16[1,2048,1024]{2,1,0:T(8,128)(2,1)} %param.26), kind=kOutput, calls=%fused_computation.23 | convolution fusion | flops 2684354560 | bytes 9437184 | tf_op jit(solution)/shard_map/dot_general | solution.py:143
  222.9 3.2 %multiply_convert_fusion = bf16[640,1024]{1,0:T(8,128)(2,1)S(1)} fusion(f32[640,1024]{1,0:T(8,128)S(1)} %fusion.15, bf16[640,2048]{1,0:T(8,128)(2,1)S(1)} %bitcast.59, bf16[1,2048,1024]{2,1,0:T(8,128)(2,1)S(1)} %copy-done.6), kind=kOutput, calls=%fused_computation.28 | convolution fusion | flops 2688286720 | bytes 10747904 | tf_op jit(solution)/shard_map/dot_general | solution.py:142
  226.1 4.2 %fusion.19 = bf16[8,80,2048]{2,1,0:T(8,128)(2,1)} fusion(bf16[8,80,1024]{2,1,0:T(8,128)(2,1)S(1)} %bitcast.61, bf16[1,1024,2048]{2,1,0:T(8,128)(2,1)S(1)} %copy-done.7), kind=kOutput, calls=%fused_computation.27 | convolution fusion | flops 2685665280 | bytes 8126464 | tf_op jit(solution)/shard_map/dot_general | solution.py:145
  230.4 34.5 %reduce-scatter.5.cloned.1.call-done = bf16[8,80,512]{2,1,0:T(8,128)(2,1)} async-done(((bf16[8,80,2048]{2,1,0:T(8,128)(2,1)}), bf16[8,80,512]{2,1,0:T(8,128)(2,1)}) %reduce-scatter.5.cloned.1.call-update) | async-done | bytes 655376 | tf_op jit(solution)/shard_map/reduce_scatter | solution.py:146
  264.9 5.5 %all-to-all-start.1 = ((bf16[8,80,512]{2,1,0:T(8,128)(2,1)}), bf16[8,80,512]{2,1,0:T(8,128)(2,1)S(1)}, u32[]{:S(2)}, u32[]{:S(2)}) async-start(bf16[8,80,512]{2,1,0:T(8,128)(2,1)} %reduce-scatter.5.cloned.1.call-done), calls=%async_computation.3 | async-start | bytes 1310720 | tf_op jit(solution)/shard_map/all_to_all | solution.py:152
  271.3 16.2 %all-to-all-done.1 = bf16[8,80,512]{2,1,0:T(8,128)(2,1)S(1)} async-done(((bf16[8,80,512]{2,1,0:T(8,128)(2,1)}), bf16[8,80,512]{2,1,0:T(8,128)(2,1)S(1)}, u32[]{:S(2)}, u32[]{:S(2)}) %all-to-all-start.1) | async-done | bytes 655392 | tf_op jit(solution)/shard_map/all_to_all | solution.py:152
  287.5 2.6 gather_fusion.1
  290.1 1.2 gather.15
  291.4 2.2 multiply_reduce_fusion
  (77 shorter events, 9.6 us)
Async XLA Ops:
  6.5 117.7 %copy-start = (bf16[512,2048]{1,0:T(8,128)(2,1)S(1)}, bf16[512,2048]{1,0:T(8,128)(2,1)}, u32[]{:S(2)}) copy-start(bf16[512,2048]{1,0:T(8,128)(2,1)} %param.21) | copy-start | bytes 6291460
  6.5 56.3 %all-gather.4.cloned.1.call-start = ((), (), s32[]{:S(2)}) async-start(), calls=%async_computation.4 | async-start | bytes 2359296 | tf_op jit(solution)/shard_map/all_gather | solution.py:66
  7.3 106.1 %all-gather.6.cloned.1.call-start = ((), (), s32[]{:S(2)}) async-start(), calls=%async_computation.5 | async-start | bytes 2359296 | tf_op jit(solution)/shard_map/all_gather | solution.py:69
  8.0 151.8 %reduce-scatter.3.cloned.1.call-start = ((), (), s32[]{:S(2)}) async-start(), calls=%async_computation.6 | async-start | bytes 1310720 | tf_op jit(solution)/shard_map/reduce_scatter | solution.py:99
  113.5 2.1 copy-start.3
  113.5 2.1 copy-start.9
  124.2 1.9 copy-start.4
  124.2 35.6 %copy-start.1 = (bf16[256,512]{1,0:T(8,128)(2,1)S(1)}, bf16[256,512]{1,0:T(8,128)(2,1)}, u32[]{:S(2)}) copy-start(bf16[256,512]{1,0:T(8,128)(2,1)} %param.16) | copy-start | bytes 786436
  126.0 91.2 %all-gather.8.cloned.1.call-start = ((), (), s32[]{:S(2)}) async-start(), calls=%async_computation.7 | async-start | bytes 3276800 | tf_op jit(solution)/shard_map/all_gather | solution.py:127
  193.9 71.0 %reduce-scatter.5.cloned.1.call-start = ((), (), s32[]{:S(2)}) async-start(), calls=%async_computation.8 | async-start | bytes 3276800 | tf_op jit(solution)/shard_map/reduce_scatter | solution.py:146
  217.3 5.6 %copy-start.6 = (bf16[1,2048,1024]{2,1,0:T(8,128)(2,1)S(1)}, bf16[1,2048,1024]{2,1,0:T(8,128)(2,1)}, u32[]{:S(2)}) copy-start(bf16[1,2048,1024]{2,1,0:T(8,128)(2,1)} %param.25) | copy-start | bytes 12582916
  217.3 5.6 %copy-start.8 = (bf16[8,80,2048]{2,1,0:T(8,128)(2,1)S(1)}, bf16[8,80,2048]{2,1,0:T(8,128)(2,1)}, u32[]{:S(2)}) copy-start(bf16[8,80,2048]{2,1,0:T(8,128)(2,1)} %all-gather.8.cloned.1.call-done) | copy-start | bytes 7864324
  222.9 3.3 %copy-start.7 = (bf16[1,1024,2048]{2,1,0:T(8,128)(2,1)S(1)}, bf16[1,1024,2048]{2,1,0:T(8,128)(2,1)}, u32[]{:S(2)}) copy-start(bf16[1,1024,2048]{2,1,0:T(8,128)(2,1)} %param.27) | copy-start | bytes 12582916
  230.3 40.8 %copy-start.5 = (f32[256,2]{0,1:T(2,128)S(1)}, f32[256,2]{0,1:T(2,128)}, u32[]{:S(2)}) copy-start(f32[256,2]{0,1:T(2,128)} %param.24) | copy-start | bytes 6148
  230.3 63.2 %copy-start.2 = (bf16[256,512]{1,0:T(8,128)(2,1)S(1)}, bf16[256,512]{1,0:T(8,128)(2,1)}, u32[]{:S(2)}) copy-start(bf16[256,512]{1,0:T(8,128)(2,1)} %reduce-scatter.3.cloned.1.call-done) | copy-start | bytes 786436
  264.9 22.6 %all-to-all-start.1 = ((bf16[8,80,512]{2,1,0:T(8,128)(2,1)}), bf16[8,80,512]{2,1,0:T(8,128)(2,1)S(1)}, u32[]{:S(2)}, u32[]{:S(2)}) async-start(bf16[8,80,512]{2,1,0:T(8,128)(2,1)} %reduce-scatter.5.cloned.1.call-done), calls=%async_computation.3 | async-start | bytes 1310720 | tf_op jit(solution)/shard_map/all_to_all | solution.py:152
Sparse Core Ops, SparseCore 0:
  9.4 53.3 all-gather.3
  64.8 48.5 all-gather.5
  126.2 33.5 reduce-scatter.2
  194.0 23.2 all-gather.7
  230.5 34.3 reduce-scatter.4
where the time goes:
time: 301 us
  waiting for transfers between devices  178 us (59%)
  blocking collectives  61.6 us (20%)
  matrix products  20.5 us (7%)
  between operations  13.4 us (4%)
  local copies, waits for them, and re-layouts  10.9 us (4%)
  other arithmetic  10.2 us (3%)
  starting transfers between devices  5.86 us (2%)
    all_gather x1, waiting for transfers between devices, shards(): lax.all_gather(values.astype(jnp.float32), 'sp', axis=1, tiled=True)  50.6 us
    reduce_scatter x1, waiting for transfers between devices, shards(): lax.psum_scatter(down_value.reshape(source_count, slot_count, model_width...  34.5 us
    all_gather x1, blocking collectives, shards(): cache_part = lax.all_gather(forget_cache, 'sp', axis=1, tiled=True)  32.8 us
    reduce_scatter x1, waiting for transfers between devices, shards(): lax.psum_scatter(projected.astype(jnp.bfloat16), 'tp', scatter_dimension=...  30.3 us
    all_gather x1, waiting for transfers between devices, shards(): lax.all_gather(lax.all_to_all(taken_rows.reshape(sp_count, capacity, norm...  23.2 us
    all_to_all x1, blocking collectives, shards(): lax.all_to_all(taken_rows.reshape(sp_count, capacity, normed.shape[1]), '...  23.1 us
    all_gather x1, waiting for transfers between devices, shards(): lax.all_gather(keys.astype(jnp.float32), 'sp', axis=1, tiled=True)  21.9 us
    all_to_all x1, waiting for transfers between devices, shards(): lax.all_to_all(summed, 'sp', split_axis=0, concat_axis=0, tiled=True)  16.2 us
  transfers between devices with their start and end apart: 6, of which 6 were waited for; matrix products, arithmetic and copies ran while one was open for 1% of the time, Pallas kernels for 0%

commit v1 on v0

v1 whole, which is shorter than its diff:
```python
import functools
import math
import jax
import jax.numpy as jnp
from jax import lax
from jax.experimental import pallas as pl
from jax.experimental.pallas import tpu as pltpu
from jax.sharding import PartitionSpec as P

norm_eps = 1e-06
masked_score = -1e30
key_span = 1024
core_pair = 2
MESH = pl.DeviceIdType.MESH


def remote(src, dst, send_sem, recv_sem, device):
    return pltpu.make_async_remote_copy(
        src_ref=src, dst_ref=dst, send_sem=send_sem, recv_sem=recv_sem,
        device_id=device, device_id_type=MESH,
    )


def greet(sp_count, tp_count):
    me, lane = lax.axis_index("sp"), lax.axis_index("tp")
    barrier = pltpu.get_barrier_semaphore()
    for step in range(1, sp_count):
        pl.semaphore_signal(
            barrier, inc=1, device_id={"sp": lax.rem(me + step, sp_count)}, device_id_type=MESH
        )
    for step in range(1, tp_count):
        pl.semaphore_signal(
            barrier, inc=1, device_id={"tp": lax.rem(lane + step, tp_count)}, device_id_type=MESH
        )
    pl.semaphore_wait(barrier, sp_count + tp_count - 2)


def attend_kernel(
    sp_count, tp_count, q_ref, k_ref, v_ref, c_ref, w_ref, r_ref,
    stream_ref, square_ref,
    q_all, k_all, v_all, c_all, k_rows, c_rows, att_out, att_in, att_rows,
    pa_out, pa_in, pb_out, pb_in, sq_out, sq_in,
    in_send, in_recv, att_send, att_recv, pa_send, pa_recv, pb_send, pb_recv, sq_send, sq_recv,
):
    n = sp_count
    me, lane = lax.axis_index("sp"), lax.axis_index("tp")
    side, row = lax.rem(lane, core_pair), lane // core_pair
    row_count = tp_count // core_pair
    head_width, block = q_ref.shape[1], q_ref.shape[2]
    local_width = r_ref.shape[1]
    partner = {"tp": row * core_pair + (core_pair - 1 - side)}
    greet(sp_count, tp_count)
    pairs = ((k_ref, k_all), (c_ref, c_all), (q_ref, q_all), (v_ref, v_all))
    started = []
    for step in range(1, n):
        peer = lax.rem(me + step, n)
        for kind, (src, dst) in enumerate(pairs):
            copy = remote(
                src.at[peer], dst.at[me], in_send.at[kind, step], in_recv.at[kind, step], {"sp": peer}
            )
            copy.start()
            started.append(copy)
    for src, dst in pairs:
        dst[me] = src[me]
    for copy in started:
        copy.wait()
    scale = head_width ** (-0.5)
    exact = float(math.log2(head_width) / 2).is_integer()
    for j in range(n):
        rows = k_all[j].astype(jnp.float32)
        if exact:
            rows = rows * scale
        k_rows[j * block : (j + 1) * block, :] = rows.T.astype(jnp.bfloat16)
        c_rows[j * block : (j + 1) * block, :] = c_all[j].T
    group = 2 if n % 2 == 0 else 1
    span = group * block

    def one_query(place):
        q = q_all[place]
        cq = c_all[place][0:1, :]
        query_place = place * block + lax.broadcasted_iota(jnp.int32, (span, block), 1)
        key_row = lax.broadcasted_iota(jnp.int32, (span, block), 0)

        def one_key(j, state):
            peak, total, acc = state
            base = pl.multiple_of(j * span, span)
            s = jnp.dot(k_rows[pl.ds(base, span), :], q, preferred_element_type=jnp.float32)
            if not exact:
                s = s * scale
            s = s + (cq - c_rows[pl.ds(base, span), 0:1])
            s = jnp.where(base + key_row <= query_place, s, masked_score)
            new_peak = jnp.maximum(peak, jnp.max(s, axis=0, keepdims=True))
            w = jnp.exp(s - new_peak)
            shrink = jnp.exp(peak - new_peak)
            total = total * shrink + jnp.sum(w, axis=0, keepdims=True)
            wb = w.astype(jnp.bfloat16)
            acc = acc * shrink
            for g in range(group):
                acc = acc + jnp.dot(
                    v_all[j * group + g], wb[g * block : (g + 1) * block, :],
                    preferred_element_type=jnp.float32,
                )
            return new_peak, total, acc

        first = (
            jnp.full((1, block), masked_score, jnp.float32),
            jnp.zeros((1, block), jnp.float32),
            jnp.zeros((head_width, block), jnp.float32),
        )
        peak, total, acc = lax.fori_loop(0, place // group + 1, one_key, first)
        return (acc / total).astype(jnp.bfloat16)

    def send_back(step):
        peer = lax.rem(me + step, n)
        return remote(
            att_out.at[step], att_in.at[me], att_send.at[step], att_recv.at[step], {"sp": peer}
        )

    def one_step(step, carry):
        att_out[step] = one_query(lax.rem(me + step, n))
        send_back(step).start()
        return carry

    lax.fori_loop(1, n, one_step, 0)
    att_in[me] = one_query(me)
    for step in range(1, n):
        send_back(step).wait()
    att_rows[...] = att_in[...].reshape(n * head_width, block).astype(jnp.float32).T.astype(jnp.bfloat16)

    def project(at):
        start = pl.multiple_of(at * local_width, local_width)
        return jnp.dot(
            att_rows[...], w_ref[:, pl.ds(start, local_width)], preferred_element_type=jnp.float32
        )

    across = []
    for r in range(row_count):
        to_row = lax.rem(row + 1 + r, row_count)
        pa_out[r] = project(to_row * core_pair + (core_pair - 1 - side)).astype(jnp.bfloat16)
        copy = remote(pa_out.at[r], pa_in.at[r], pa_send.at[r], pa_recv.at[r], partner)
        copy.start()
        across.append(copy)
    along = []
    for r in range(row_count - 1):
        to_row = lax.rem(row + 1 + r, row_count)
        part = project(to_row * core_pair + side)
        across[r].wait()
        pb_out[r] = (part + pa_in[r].astype(jnp.float32)).astype(jnp.bfloat16)
        copy = remote(
            pb_out.at[r], pb_in.at[r], pb_send.at[r], pb_recv.at[r], {"tp": to_row * core_pair + side}
        )
        copy.start()
        along.append(copy)
    part = project(lane)
    across[row_count - 1].wait()
    part = part + pa_in[row_count - 1].astype(jnp.float32) + r_ref[...].astype(jnp.float32)
    for r in range(row_count - 1):
        along[r].wait()
        part = part + pb_in[r].astype(jnp.float32)
    stream = part.astype(jnp.bfloat16)
    stream_ref[...] = stream
    wide = stream.astype(jnp.float32)
    own = lax.dot_general(
        jnp.ones((8, local_width), jnp.float32), wide * wide, (((1,), (1,)), ((), ())),
        preferred_element_type=jnp.float32, precision=lax.Precision.HIGHEST,
    )
    sq_out[...] = own
    sums = []
    for step in range(1, tp_count):
        copy = remote(
            sq_out, sq_in.at[step], sq_send.at[step], sq_recv.at[step],
            {"tp": lax.rem(lane + step, tp_count)},
        )
        copy.start()
        sums.append(copy)
    for step in range(1, tp_count):
        sums[step - 1].wait()
        own = own + sq_in[step]
    square_ref[...] = own


def dispatch_kernel(
    sp_count, tp_count, t_ref, arr_ref, a_send, a_recv, y_send, y_recv, c_send, c_recv
):
    n = sp_count
    me, lane = lax.axis_index("sp"), lax.axis_index("tp")
    side, row = lax.rem(lane, core_pair), lane // core_pair
    row_count = tp_count // core_pair
    width = t_ref.shape[2]
    partner = {"tp": row * core_pair + (core_pair - 1 - side)}

    def part(source, at):
        return arr_ref.at[source, :, pl.ds(pl.multiple_of(at * width, width), width)]

    greet(sp_count, tp_count)
    entry = [None]
    for step in range(1, n):
        peer = lax.rem(me + step, n)
        copy = remote(t_ref.at[peer], part(me, lane), a_send.at[step], a_recv.at[step], {"sp": peer})
        copy.start()
        entry.append(copy)
    waits, rows = [], []
    for step in range(n):
        source = lax.rem(me + n - step, n)
        if step == 0:
            mine = t_ref.at[me]
        else:
            entry[step].wait()
            mine = part(source, lane)
        if step == 0:
            arr_ref[me, :, pl.ds(pl.multiple_of(lane * width, width), width)] = t_ref[me]
        for r in range(row_count - 1):
            to_row = lax.rem(row + 1 + r, row_count)
            copy = remote(
                mine, part(source, lane), y_send.at[r, step], y_recv.at[r, step],
                {"tp": to_row * core_pair + side},
            )
            copy.start()
            rows.append((r, step, source, copy))
        copy = remote(mine, part(source, lane), c_send.at[0, step], c_recv.at[0, step], partner)
        copy.start()
        waits.append(copy)
    for r, step, source, copy in rows:
        copy.wait()
        from_row = lax.rem(row + row_count - 1 - r, row_count)
        block = part(source, from_row * core_pair + side)
        onward = remote(block, block, c_send.at[1 + r, step], c_recv.at[1 + r, step], partner)
        onward.start()
        waits.append(onward)
    for copy in waits:
        copy.wait()


def collect_kernel(
    sp_count, tp_count, d_ref, back_ref, pa_in, pb_out, pb_in, fin,
    pa_send, pa_recv, pb_send, pb_recv, f_send, f_recv
):
    n = sp_count
    me, lane = lax.axis_index("sp"), lax.axis_index("tp")
    side, row = lax.rem(lane, core_pair), lane // core_pair
    row_count = tp_count // core_pair
    width = back_ref.shape[2]
    partner = {"tp": row * core_pair + (core_pair - 1 - side)}

    def columns(at):
        return pl.ds(pl.multiple_of(at * width, width), width)

    greet(sp_count, tp_count)
    homes = [lax.rem(me + 1 + k, n) for k in range(n)]
    across, along, final = {}, {}, []
    for k in range(n):
        for r in range(row_count):
            to_row = lax.rem(row + 1 + r, row_count)
            at = to_row * core_pair + (core_pair - 1 - side)
            copy = remote(
                d_ref.at[homes[k], :, columns(at)], pa_in.at[r, k],
                pa_send.at[r, k], pa_recv.at[r, k], partner,
            )
            copy.start()
            across[r, k] = copy
    for k in range(n):
        for r in range(row_count - 1):
            at = lax.rem(row + 1 + r, row_count) * core_pair + side
            across[r, k].wait()
            held = d_ref[homes[k], :, columns(at)].astype(jnp.float32)
            pb_out[r, k] = (held + pa_in[r, k].astype(jnp.float32)).astype(jnp.bfloat16)
            copy = remote(
                pb_out.at[r, k], pb_in.at[r, k], pb_send.at[r, k], pb_recv.at[r, k], {"tp": at}
            )
            copy.start()
            along[r, k] = copy
    for k in range(n):
        across[row_count - 1, k].wait()
        total = d_ref[homes[k], :, columns(lane)].astype(jnp.float32)
        total = total + pa_in[row_count - 1, k].astype(jnp.float32)
        for r in range(row_count - 1):
            along[r, k].wait()
            total = total + pb_in[r, k].astype(jnp.float32)
        if k < n - 1:
            fin[k] = total.astype(jnp.bfloat16)
            copy = remote(fin.at[k], back_ref.at[me], f_send.at[k], f_recv.at[k], {"sp": homes[k]})
            copy.start()
            final.append(copy)
        else:
            back_ref[me] = total.astype(jnp.bfloat16)
    for copy in final:
        copy.wait()


def dma(*shape):
    return pltpu.SemaphoreType.DMA(shape)


def vmem_specs(count):
    return [pl.BlockSpec(memory_space=pltpu.VMEM)] * count


def params(number):
    return pltpu.CompilerParams(
        collective_id=number, has_side_effects=True, vmem_limit_bytes=50 * 1024 * 1024
    )


def fast_attention(residual, queries, keys, values, forget_cache, out_weight, sp_count, tp_count):
    token_count, local_width = residual.shape
    head_count = forget_cache.shape[0]
    head_width = queries.shape[0] // head_count
    heads = (head_count, head_width, token_count)
    cache = jnp.broadcast_to(forget_cache[:, None, :], (head_count, 8, token_count))
    row_count = tp_count // core_pair
    half, full = jnp.bfloat16, jnp.float32
    block = (token_count, local_width)
    return pl.pallas_call(
        functools.partial(attend_kernel, sp_count, tp_count),
        out_shape=(
            jax.ShapeDtypeStruct(block, half),
            jax.ShapeDtypeStruct((8, token_count), full),
        ),
        in_specs=vmem_specs(6),
        out_specs=tuple(vmem_specs(2)),
        scratch_shapes=[
            pltpu.VMEM(heads, half),
            pltpu.VMEM(heads, half),
            pltpu.VMEM(heads, half),
            pltpu.VMEM((sp_count, 8, token_count), full),
            pltpu.VMEM((sp_count * token_count, head_width), half),
            pltpu.VMEM((sp_count * token_count, 8), full),
            pltpu.VMEM(heads, half),
            pltpu.VMEM(heads, half),
            pltpu.VMEM((token_count, head_count * head_width), half),
            pltpu.VMEM((row_count,) + block, half),
            pltpu.VMEM((row_count,) + block, half),
            pltpu.VMEM((row_count,) + block, half),
            pltpu.VMEM((row_count,) + block, half),
            pltpu.VMEM((8, token_count), full),
            pltpu.VMEM((tp_count, 8, token_count), full),
            dma(4, sp_count), dma(4, sp_count), dma(sp_count), dma(sp_count),
            dma(row_count), dma(row_count), dma(row_count), dma(row_count),
            dma(tp_count), dma(tp_count),
        ],
        compiler_params=params(0),
    )(queries.reshape(heads), keys.reshape(heads), values.reshape(heads), cache, out_weight, residual)


def fast_dispatch(taken, sp_count, tp_count, model_width):
    capacity = taken.shape[1]
    row_count = tp_count // core_pair
    return pl.pallas_call(
        functools.partial(dispatch_kernel, sp_count, tp_count),
        out_shape=jax.ShapeDtypeStruct((sp_count, capacity, model_width), jnp.bfloat16),
        in_specs=vmem_specs(1),
        out_specs=vmem_specs(1)[0],
        scratch_shapes=[
            dma(sp_count), dma(sp_count), dma(row_count, sp_count), dma(row_count, sp_count),
            dma(row_count, sp_count), dma(row_count, sp_count),
        ],
        compiler_params=params(1),
    )(taken)


def fast_collect(down, sp_count, tp_count):
    capacity, local_width = down.shape[1], down.shape[2] // tp_count
    row_count = tp_count // core_pair
    piece = (sp_count, capacity, local_width)
    half = jnp.bfloat16
    return pl.pallas_call(
        functools.partial(collect_kernel, sp_count, tp_count),
        out_shape=jax.ShapeDtypeStruct(piece, half),
        in_specs=vmem_specs(1),
        out_specs=vmem_specs(1)[0],
        scratch_shapes=[
            pltpu.VMEM((row_count,) + piece, half),
            pltpu.VMEM((row_count,) + piece, half),
            pltpu.VMEM((row_count,) + piece, half),
            pltpu.VMEM(piece, half),
            dma(row_count, sp_count), dma(row_count, sp_count),
            dma(row_count, sp_count), dma(row_count, sp_count),
            dma(sp_count), dma(sp_count),
        ],
        compiler_params=params(2),
    )(down)


def ring_attention(
    residual,
    queries,
    keys,
    values,
    forget_cache,
    out_weight,
):
    sp_count = lax.axis_size("sp")
    token_count = residual.shape[0]
    head_count = forget_cache.shape[0]
    head_width = queries.shape[0] // head_count
    first_token = lax.axis_index("sp") * token_count
    last_token = first_token + token_count - 1
    query_heads = queries.reshape(head_count, head_width, token_count)
    query_place = first_token + jnp.arange(token_count, dtype=jnp.int32)
    score_scale = head_width ** (-0.5)

    def attend_block(state_now, key_block, value_block, cache_block, key_first):
        running_peak, running_total, running_sum = state_now
        block_length = key_block.shape[1]
        key_heads = key_block.reshape(head_count, head_width, block_length)
        value_heads = value_block.reshape(head_count, head_width, block_length)
        scores = (
            jnp.einsum("hdq,hdk->hqk", query_heads, key_heads, preferred_element_type=jnp.float32)
            * score_scale
        )
        scores = scores + forget_cache[:, :, None] - cache_block[:, None, :]
        key_place = key_first + jnp.arange(block_length, dtype=jnp.int32)
        allowed = key_place[None, :] <= query_place[:, None]
        scores = jnp.where(allowed[None], scores, masked_score)
        new_peak = jnp.maximum(running_peak, jnp.max(scores, axis=2))
        weights = jnp.exp(scores - new_peak[:, :, None])
        shrink = jnp.exp(running_peak - new_peak)
        new_total = running_total * shrink + jnp.sum(weights, axis=2)
        new_sum = running_sum * shrink[:, None, :] + jnp.einsum(
            "hdk,hqk->hdq",
            value_heads,
            weights.astype(jnp.bfloat16),
            preferred_element_type=jnp.float32,
        )
        return (new_peak, new_total, new_sum)

    initial = (
        jnp.full((head_count, token_count), masked_score, jnp.float32),
        jnp.zeros((head_count, token_count), jnp.float32),
        jnp.zeros((head_count, head_width, token_count), jnp.float32),
    )
    key_part = lax.all_gather(keys.astype(jnp.float32), "sp", axis=1, tiled=True).astype(
        jnp.bfloat16
    )
    value_part = lax.all_gather(values.astype(jnp.float32), "sp", axis=1, tiled=True).astype(
        jnp.bfloat16
    )
    cache_part = lax.all_gather(forget_cache, "sp", axis=1, tiled=True)
    part_length = key_part.shape[1]
    block_length = key_span

    def one_block(block_index, state_in):
        start_column = block_index * block_length
        key_block = lax.dynamic_slice_in_dim(key_part, start_column, block_length, 1)
        value_block = lax.dynamic_slice_in_dim(value_part, start_column, block_length, 1)
        cache_block = lax.dynamic_slice_in_dim(cache_part, start_column, block_length, 1)
        return lax.cond(
            start_column <= last_token,
            lambda inner: attend_block(inner, key_block, value_block, cache_block, start_column),
            lambda inner: inner,
            state_in,
        )

    final_peak, final_total, final_sum = lax.fori_loop(
        0, part_length // block_length, one_block, initial
    )
    attended = (
        (final_sum / final_total[:, None, :])
        .astype(jnp.bfloat16)
        .reshape(head_count * head_width, token_count)
    )
    projected = lax.dot_general(
        attended, out_weight, (((0,), (0,)), ((), ())), preferred_element_type=jnp.float32
    )
    head_sum = lax.psum_scatter(
        projected.astype(jnp.bfloat16), "tp", scatter_dimension=1, tiled=True
    ).astype(jnp.float32)
    stream = (residual.astype(jnp.float32) + head_sum).astype(jnp.bfloat16)
    local_rows = stream.astype(jnp.float32)
    return stream, lax.psum(jnp.sum(local_rows * local_rows, axis=1), "tp")


def shards(
    residual,
    queries,
    keys,
    values,
    forget_cache,
    out_weight,
    norm_gain,
    routes,
    route_weight,
    gate_weight,
    up_weight,
    down_weight,
):
    sp_count, tp_count = lax.axis_size("sp"), lax.axis_size("tp")
    token_count, local_width = residual.shape
    model_width = norm_gain.shape[0]
    top_count = routes.shape[1]
    item_count = token_count * top_count
    capacity = max(2, token_count * top_count * 5 // (4 * sp_count))
    slot_total = sp_count * capacity
    paired = tp_count % core_pair == 0 and tp_count > core_pair and local_width % 128 == 0
    head_count = forget_cache.shape[0]
    if paired and head_count == sp_count:
        stream, squares = fast_attention(
            residual, queries, keys, values, forget_cache, out_weight, sp_count, tp_count
        )
        squares = squares[0]
    else:
        stream, squares = ring_attention(residual, queries, keys, values, forget_cache, out_weight)
    local_rows = stream.astype(jnp.float32)
    expert_of = routes.reshape(item_count)
    onehot = (expert_of[:, None] == jnp.arange(sp_count, dtype=jnp.int32)[None, :]).astype(
        jnp.int32
    )
    earlier = jnp.cumsum(onehot, axis=0) - onehot
    target = (expert_of * capacity + jnp.sum(earlier * onehot, axis=1)).reshape(
        token_count, top_count
    )
    slots = jnp.arange(slot_total, dtype=jnp.int32)
    row_scale = lax.rsqrt(squares / model_width + norm_eps)
    local_gain = lax.dynamic_slice_in_dim(
        norm_gain, lax.axis_index("tp") * local_width, local_width
    )
    normed = (local_rows * row_scale[:, None] * local_gain[None, :]).astype(jnp.bfloat16)
    pick = jnp.any(target.T[:, None, :] == slots[None, :, None], axis=0).astype(jnp.bfloat16)
    taken_rows = (
        jnp.dot(pick, normed, preferred_element_type=jnp.float32)
        .astype(jnp.bfloat16)
        .reshape(sp_count, capacity, local_width)
    )
    direct = paired and capacity % 16 == 0
    if direct:
        arrived = fast_dispatch(taken_rows, sp_count, tp_count, model_width)
    else:
        arrived = lax.all_gather(
            lax.all_to_all(taken_rows, "sp", split_axis=0, concat_axis=0, tiled=True),
            "tp",
            axis=2,
            tiled=True,
        )
    flat_rows = arrived.reshape(slot_total, model_width)
    gate_value = jnp.dot(flat_rows, gate_weight[0], preferred_element_type=jnp.float32)
    up_value = jnp.dot(flat_rows, up_weight[0], preferred_element_type=jnp.float32)
    hidden = (jax.nn.silu(gate_value) * up_value).astype(jnp.bfloat16)
    down_value = (
        jnp.dot(hidden, down_weight[0], preferred_element_type=jnp.float32)
        .astype(jnp.bfloat16)
        .reshape(sp_count, capacity, model_width)
    )
    if direct:
        expert_back = fast_collect(down_value, sp_count, tp_count)
    else:
        summed = lax.psum_scatter(down_value, "tp", scatter_dimension=2, tiled=True)
        expert_back = lax.all_to_all(summed, "sp", split_axis=0, concat_axis=0, tiled=True)
    back_rows = expert_back.reshape(slot_total, local_width)
    share = jnp.sum(
        jnp.where(target[:, :, None] == slots[None, None, :], route_weight[:, :, None], 0.0), axis=1
    )
    share_high = share.astype(jnp.bfloat16)
    share_low = (share - share_high.astype(jnp.float32)).astype(jnp.bfloat16)
    mixture = jnp.dot(share_high, back_rows, preferred_element_type=jnp.float32) + jnp.dot(
        share_low, back_rows, preferred_element_type=jnp.float32
    )
    return (local_rows + mixture).astype(jnp.bfloat16)


def solution(mesh):
    return jax.shard_map(
        shards,
        mesh=mesh,
        in_specs=(
            P("sp", "tp"),
            P("tp", "sp"),
            P("tp", "sp"),
            P("tp", "sp"),
            P("tp", "sp"),
            P("tp", None),
            P(),
            P("sp", None),
            P("sp", None),
            P("sp", None, "tp"),
            P("sp", None, "tp"),
            P("sp", "tp", None),
        ),
        out_specs=P("sp", "tp"),
        check_vma=False,
    )
```

time: 301 us -> 135 us (0.45)
  waiting for transfers between devices: 178 us -> 0 us
  Pallas kernels: 0 us -> 104 us
  blocking collectives: 61.6 us -> 0 us
  between operations: 13.4 us -> 0.12 us
  other arithmetic: 10.2 us -> 2.41 us
  starting transfers between devices: 5.86 us -> 0 us
    pallas_call x0 -> x3, Pallas kernels: none -> 104 us  [the longest x1 51.1 us: fast_attention(): pl.pallas_call(functools.partial(attend_kernel, sp_count, tp_count), out_...]
    all_gather x3 -> x0, waiting for transfers between devices: 95.7 us -> none  [the longest x1 50.6 us: shards(): lax.all_gather(values.astype(jnp.float32), 'sp', axis=1, tiled=True)]
    reduce_scatter x2 -> x0, waiting for transfers between devices: 64.8 us -> none  [the longest x1 34.5 us: shards(): lax.psum_scatter(down_value.reshape(source_count, slot_count, model_width...]
    all_gather x1 -> x0, blocking collectives: 32.8 us -> none  [shards(): cache_part = lax.all_gather(forget_cache, 'sp', axis=1, tiled=True)]
    all_to_all x1 -> x0, blocking collectives: 23.1 us -> none  [shards(): lax.all_to_all(taken_rows.reshape(sp_count, capacity, normed.shape[1]), '...]
    all_to_all x1 -> x0, waiting for transfers between devices: 16.2 us -> none  [shards(): lax.all_to_all(summed, 'sp', split_axis=0, concat_axis=0, tiled=True)]
    dot_general x4 -> x3, matrix products: 10.7 us -> 1.88 us  [the longest x1 1.08 us: shards(): jnp.dot(share_low, back_rows, preferred_element_type=jnp.float32)]
    unnamed x18 -> x17, local copies, waits for them, and re-layouts: 0.3 us -> 7.95 us
  transfers between devices with their start and end apart: 6 -> 0, of which waited for: 6 -> 0; matrix products, arithmetic and copies ran while one was open for 1% -> 0% of each run, Pallas kernels for 0% -> 0%
where the time goes in v1:
time: 135 us; the launch traced here: 134 us
  Pallas kernels  104 us (77%)
  matrix products  17.8 us (13%)
  local copies, waits for them, and re-layouts  10.1 us (7%)
  other arithmetic  2.41 us (2%)
    pallas_call x1, Pallas kernels, fast_attention(): pl.pallas_call(functools.partial(attend_kernel, sp_count, tp_count), out_...  51.1 us
    pallas_call x1, Pallas kernels, fast_collect(): pl.pallas_call(functools.partial(collect_kernel, sp_count, tp_count), out...  28.6 us
    pallas_call x1, Pallas kernels, fast_dispatch(): pl.pallas_call(functools.partial(dispatch_kernel, sp_count, tp_count), ou...  24 us
    dot_general x1, matrix products, shards(): jnp.dot(hidden, down_weight[0], preferred_element_type=jnp.float32)  11.6 us
    unnamed x17, local copies, waits for them, and re-layouts  7.95 us
    dot_general x1, matrix products, shards(): jnp.dot(flat_rows, up_weight[0], preferred_element_type=jnp.float32)  4.38 us

profile of v1, /device:TPU:0, one launch (start us, length us, event | category | flops | bytes accessed | tf_op | source)
XLA Modules:
  0.0 134.1 jit_solution(9178612876675236142)
XLA Ops:
  0.0 0.8 copy.27
  1.0 1.1 reduce-window.6
  2.1 0.2 slice_reduce_fusion
  2.4 0.1 eq.51
  2.6 0.1 reduce_sum.21
  2.8 0.7 multiply_add_fusion
  3.5 0.2 fusion.11
  3.8 0.8 dynamic_slice.3
  4.5 0.7 broadcast_in_dim.10.c_ref
  5.2 1.6 %copy-done.1 = bf16[512,2048]{1,0:T(8,128)(2,1)S(1)} copy-done((bf16[512,2048]{1,0:T(8,128)(2,1)S(1)}, bf16[512,2048]{1,0:T(8,128)(2,1)}, u32[]{:S(2)}) %copy-start.1) | copy-done | bytes 2097176
  6.8 0.9 copy-done.2
  7.8 0.9 copy-done.3
  8.7 0.9 copy-done.4
  9.7 0.9 copy-done.5
  10.6 51.1 %shard_map.118 = (bf16[256,512]{1,0:T(8,128)(2,1)S(1)}, f32[8,256]{1,0:T(8,128)S(1)}) custom-call(bf16[8,64,256]{2,1,0:T(8,128)(2,1)S(1)} %bitcast.43, bf16[8,64,256]{2,1,0:T(8,128)(2,1)S(1)} %bitcast.44, bf16[8,64,256]{2,1,0:T(8,128)(2,1)S(1)} %bitcast.45, f32[8,8,256]{2,1,0:T(8,128)S(1)} %broadcast_in_dim.10.c_ref, bf16[512,2048]{1,0:T(8,128)(2,1)S(1)} %copy-done.1, ...), custom_call_target="tpu_custom_call" | custom-call | tf_op jit(solution)/shard_map/pallas_call | solution.py:313
  61.7 0.4 convolution_convert_fusion
  62.2 24.0 %shard_map.119 = bf16[8,80,2048]{2,1,0:T(8,128)(2,1)S(1)} custom-call(bf16[8,80,512]{2,1,0:T(8,128)(2,1)S(1)} %bitcast.42), custom_call_target="tpu_custom_call" | custom-call | tf_op jit(solution)/shard_map/pallas_call | solution.py:348
  86.2 4.4 %fusion.2 = f32[640,1024]{1,0:T(8,128)} fusion(bf16[640,2048]{1,0:T(8,128)(2,1)S(1)} %bitcast.39, bf16[1,2048,1024]{2,1,0:T(8,128)(2,1)S(1)} %copy-done.7), kind=kOutput, calls=%fused_computation.2 | convolution fusion | flops 2684354560 | bytes 9437184 | tf_op jit(solution)/shard_map/dot_general | solution.py:536
  90.5 11.6 %fusion.6 = bf16[640,2048]{1,0:T(8,128)(2,1)} fusion(bf16[1,1024,2048]{2,1,0:T(8,128)(2,1)} %param.23, f32[640,1024]{1,0:T(8,128)} %fusion.2, bf16[640,2048]{1,0:T(8,128)(2,1)S(1)} %bitcast.40, bf16[1,2048,1024]{2,1,0:T(8,128)(2,1)} %param.21), kind=kOutput, calls=%fused_computation.6 | convolution fusion | flops 5373952000 | bytes 16252928 | tf_op jit(solution)/shard_map/dot_general | solution.py:539
  102.1 1.7 %copy-done = bf16[640,2048]{1,0:T(8,128)(2,1)S(1)} copy-done((bf16[640,2048]{1,0:T(8,128)(2,1)S(1)}, bf16[640,2048]{1,0:T(8,128)(2,1)}, u32[]{:S(2)}) %copy-start) | copy-done | bytes 2621464
  103.9 28.6 %shard_map.120 = bf16[8,80,512]{2,1,0:T(8,128)(2,1)S(1)} custom-call(bf16[8,80,2048]{2,1,0:T(8,128)(2,1)S(1)} %bitcast.41), custom_call_target="tpu_custom_call" | custom-call | tf_op jit(solution)/shard_map/pallas_call | solution.py:366
  132.4 0.2 select_reduce_fusion
  132.6 0.4 fusion.22
  133.0 1.1 fusion.13
  (17 shorter events, 0.4 us)
Async XLA Ops:
  5.2 1.6 %copy-start.1 = (bf16[512,2048]{1,0:T(8,128)(2,1)S(1)}, bf16[512,2048]{1,0:T(8,128)(2,1)}, u32[]{:S(2)}) copy-start(bf16[512,2048]{1,0:T(8,128)(2,1)} %w_ref.1) | copy-start | bytes 6291460
  6.8 0.9 copy-start.2
  7.8 0.9 copy-start.3
  8.7 0.9 copy-start.4
  9.7 0.9 copy-start.5
  61.7 24.4 %copy-start.7 = (bf16[1,2048,1024]{2,1,0:T(8,128)(2,1)S(1)}, bf16[1,2048,1024]{2,1,0:T(8,128)(2,1)}, u32[]{:S(2)}) copy-start(bf16[1,2048,1024]{2,1,0:T(8,128)(2,1)} %param.22) | copy-start | bytes 12582916
  102.1 1.7 %copy-start = (bf16[640,2048]{1,0:T(8,128)(2,1)S(1)}, bf16[640,2048]{1,0:T(8,128)(2,1)}, u32[]{:S(2)}) copy-start(bf16[640,2048]{1,0:T(8,128)(2,1)} %fusion.6) | copy-start | bytes 7864324
  103.9 28.6 %copy-start.6 = (f32[256,2]{0,1:T(2,128)S(1)}, f32[256,2]{0,1:T(2,128)}, u32[]{:S(2)}) copy-start(f32[256,2]{0,1:T(2,128)} %param.20) | copy-start | bytes 6148

commit v2 on v1

--- a/solution.py
+++ b/solution.py
@@ -36,8 +36,9 @@
 
 
 def attend_kernel(
-    sp_count, tp_count, q_ref, k_ref, v_ref, c_ref, w_ref, r_ref,
+    sp_count, tp_count, q_hbm, k_hbm, v_hbm, c_ref, w_hbm, r_hbm,
     stream_ref, square_ref,
+    q_ref, k_ref, v_ref, w_ref, r_ref, load_sem,
     q_all, k_all, v_all, c_all, k_rows, c_rows, att_out, att_in, att_rows,
     pa_out, pa_in, pb_out, pb_in, sq_out, sq_in,
     in_send, in_recv, att_send, att_recv, pa_send, pa_recv, pb_send, pb_recv, sq_send, sq_recv,
@@ -49,7 +50,15 @@
     head_width, block = q_ref.shape[1], q_ref.shape[2]
     local_width = r_ref.shape[1]
     partner = {"tp": row * core_pair + (core_pair - 1 - side)}
+    loads = []
+    for at, (src, dst) in enumerate(
+        ((k_hbm, k_ref), (q_hbm, q_ref), (v_hbm, v_ref), (w_hbm, w_ref), (r_hbm, r_ref))
+    ):
+        loads.append(pltpu.make_async_copy(src, dst, load_sem.at[at]))
+        loads[at].start()
     greet(sp_count, tp_count)
+    for at in range(3):
+        loads[at].wait()
     pairs = ((k_ref, k_all), (c_ref, c_all), (q_ref, q_all), (v_ref, v_all))
     started = []
     for step in range(1, n):
@@ -127,6 +136,9 @@
         send_back(step).wait()
     att_rows[...] = att_in[...].reshape(n * head_width, block).astype(jnp.float32).T.astype(jnp.bfloat16)
 
+    for at in range(3, 5):
+        loads[at].wait()
+
     def project(at):
         start = pl.multiple_of(at * local_width, local_width)
         return jnp.dot(
@@ -179,110 +191,151 @@
     square_ref[...] = own
 
 
-def dispatch_kernel(
-    sp_count, tp_count, t_ref, arr_ref, a_send, a_recv, y_send, y_recv, c_send, c_recv
-):
-    n = sp_count
-    me, lane = lax.axis_index("sp"), lax.axis_index("tp")
-    side, row = lax.rem(lane, core_pair), lane // core_pair
-    row_count = tp_count // core_pair
-    width = t_ref.shape[2]
-    partner = {"tp": row * core_pair + (core_pair - 1 - side)}
-
-    def part(source, at):
-        return arr_ref.at[source, :, pl.ds(pl.multiple_of(at * width, width), width)]
-
-    greet(sp_count, tp_count)
-    entry = [None]
-    for step in range(1, n):
-        peer = lax.rem(me + step, n)
-        copy = remote(t_ref.at[peer], part(me, lane), a_send.at[step], a_recv.at[step], {"sp": peer})
-        copy.start()
-        entry.append(copy)
-    waits, rows = [], []
-    for step in range(n):
-        source = lax.rem(me + n - step, n)
-        if step == 0:
-            mine = t_ref.at[me]
-        else:
-            entry[step].wait()
-            mine = part(source, lane)
-        if step == 0:
-            arr_ref[me, :, pl.ds(pl.multiple_of(lane * width, width), width)] = t_ref[me]
-        for r in range(row_count - 1):
-            to_row = lax.rem(row + 1 + r, row_count)
-            copy = remote(
-                mine, part(source, lane), y_send.at[r, step], y_recv.at[r, step],
-                {"tp": to_row * core_pair + side},
-            )
-            copy.start()
-            rows.append((r, step, source, copy))
-        copy = remote(mine, part(source, lane), c_send.at[0, step], c_recv.at[0, step], partner)
-        copy.start()
-        waits.append(copy)
-    for r, step, source, copy in rows:
-        copy.wait()
-        from_row = lax.rem(row + row_count - 1 - r, row_count)
-        block = part(source, from_row * core_pair + side)
-        onward = remote(block, block, c_send.at[1 + r, step], c_recv.at[1 + r, step], partner)
-        onward.start()
-        waits.append(onward)
-    for copy in waits:
-        copy.wait()
-
-
-def collect_kernel(
-    sp_count, tp_count, d_ref, back_ref, pa_in, pb_out, pb_in, fin,
+def expert_kernel(
+    sp_count, tp_count, t_ref, g_hbm, u_hbm, d_hbm, back_ref,
+    g_ref, u_ref, d_ref, arr, hid, down, pa_in, pb_out, pb_in, fin,
+    load_sem, a_send, a_recv, y_send, y_recv, c_send, c_recv,
     pa_send, pa_recv, pb_send, pb_recv, f_send, f_recv
 ):
     n = sp_count
     me, lane = lax.axis_index("sp"), lax.axis_index("tp")
     side, row = lax.rem(lane, core_pair), lane // core_pair
     row_count = tp_count // core_pair
-    width = back_ref.shape[2]
+    capacity, width = t_ref.shape[1], t_ref.shape[2]
+    model_width, hidden_width = g_ref.shape
     partner = {"tp": row * core_pair + (core_pair - 1 - side)}
+    loads = []
+    for at, (src, dst) in enumerate(((g_hbm, g_ref), (u_hbm, u_ref), (d_hbm, d_ref))):
+        loads.append(pltpu.make_async_copy(src.at[0], dst, load_sem.at[at]))
+        loads[at].start()
 
     def columns(at):
         return pl.ds(pl.multiple_of(at * width, width), width)
 
+    def part(step, at):
+        return arr.at[step, :, columns(at)]
+
     greet(sp_count, tp_count)
-    homes = [lax.rem(me + 1 + k, n) for k in range(n)]
-    across, along, final = {}, {}, []
-    for k in range(n):
-        for r in range(row_count):
+    entry = [None]
+    for step in range(1, n):
+        peer = lax.rem(me + step, n)
+        copy = remote(t_ref.at[peer], part(step, lane), a_send.at[step], a_recv.at[step], {"sp": peer})
+        copy.start()
+        entry.append(copy)
+    homes = [lax.rem(me + n - k, n) for k in range(n)]
+    sides, rows, across, along, final = {}, {}, {}, {}, []
+
+    def forward(step):
+        if step == 0:
+            arr[0, :, columns(lane)] = t_ref[me]
+            mine = t_ref.at[me]
+        else:
+            entry[step].wait()
+            mine = part(step, lane)
+        for r in range(row_count - 1):
             to_row = lax.rem(row + 1 + r, row_count)
-            at = to_row * core_pair + (core_pair - 1 - side)
-            copy = remote(
-                d_ref.at[homes[k], :, columns(at)], pa_in.at[r, k],
-                pa_send.at[r, k], pa_recv.at[r, k], partner,
+            rows[r, step] = remote(
+                mine, part(step, lane), y_send.at[r, step], y_recv.at[r, step],
+                {"tp": to_row * core_pair + side},
             )
-            copy.start()
-            across[r, k] = copy
-    for k in range(n):
+            rows[r, step].start()
+        sides[0, step] = remote(
+            mine, part(step, lane), c_send.at[0, step], c_recv.at[0, step], partner
+        )
+        sides[0, step].start()
+
+    def relay(step):
+        for r in range(row_count - 1):
+            rows[r, step].wait()
+            from_row = lax.rem(row + row_count - 1 - r, row_count)
+            block = part(step, from_row * core_pair + side)
+            sides[1 + r, step] = remote(
+                block, block, c_send.at[1 + r, step], c_recv.at[1 + r, step], partner
+            )
+            sides[1 + r, step].start()
+
+    def tile_of(total):
+        return 256 if total % 256 == 0 else 128
+
+    hidden_tile, down_tile = tile_of(hidden_width), tile_of(model_width)
+
+    def compute(first, count):
+        for step in range(first, first + count):
+            for r in range(row_count):
+                sides[r, step].wait()
+        height = count * capacity
+        if first == 0:
+            for load in loads:
+                load.wait()
+
+        def one_hidden(f, carry):
+            at = pl.ds(pl.multiple_of(f * hidden_tile, hidden_tile), hidden_tile)
+            x = arr[first : first + count].reshape(height, model_width)
+            gate = jnp.dot(x, g_ref[:, at], preferred_element_type=jnp.float32)
+            up = jnp.dot(x, u_ref[:, at], preferred_element_type=jnp.float32)
+            value = (gate / (1.0 + jnp.exp(-gate))) * up
+            hid[0:height, at] = value.astype(jnp.bfloat16)
+            return carry
+
+        lax.fori_loop(0, hidden_width // hidden_tile, one_hidden, 0)
+
+        def one_down(f, carry):
+            at = pl.ds(pl.multiple_of(f * down_tile, down_tile), down_tile)
+            value = jnp.dot(hid[0:height, :], d_ref[:, at], preferred_element_type=jnp.float32)
+            down[first : first + count, :, at] = value.astype(jnp.bfloat16).reshape(
+                count, capacity, down_tile
+            )
+            return carry
+
+        lax.fori_loop(0, model_width // down_tile, one_down, 0)
+        for k in range(first, first + count):
+            for r in range(row_count):
+                to_row = lax.rem(row + 1 + r, row_count)
+                at = to_row * core_pair + (core_pair - 1 - side)
+                across[r, k] = remote(
+                    down.at[k, :, columns(at)], pa_in.at[r, k],
+                    pa_send.at[r, k], pa_recv.at[r, k], partner,
+                )
+                across[r, k].start()
+
+    def exchange(k):
         for r in range(row_count - 1):
             at = lax.rem(row + 1 + r, row_count) * core_pair + side
             across[r, k].wait()
-            held = d_ref[homes[k], :, columns(at)].astype(jnp.float32)
+            held = down[k, :, columns(at)].astype(jnp.float32)
             pb_out[r, k] = (held + pa_in[r, k].astype(jnp.float32)).astype(jnp.bfloat16)
-            copy = remote(
+            along[r, k] = remote(
                 pb_out.at[r, k], pb_in.at[r, k], pb_send.at[r, k], pb_recv.at[r, k], {"tp": at}
             )
-            copy.start()
-            along[r, k] = copy
-    for k in range(n):
+            along[r, k].start()
+
+    def finish(k):
         across[row_count - 1, k].wait()
-        total = d_ref[homes[k], :, columns(lane)].astype(jnp.float32)
+        total = down[k, :, columns(lane)].astype(jnp.float32)
         total = total + pa_in[row_count - 1, k].astype(jnp.float32)
         for r in range(row_count - 1):
             along[r, k].wait()
             total = total + pb_in[r, k].astype(jnp.float32)
-        if k < n - 1:
+        if k > 0:
             fin[k] = total.astype(jnp.bfloat16)
             copy = remote(fin.at[k], back_ref.at[me], f_send.at[k], f_recv.at[k], {"sp": homes[k]})
             copy.start()
             final.append(copy)
         else:
             back_ref[me] = total.astype(jnp.bfloat16)
+
+    count = 2 if n % 2 == 0 else 1
+    groups = n // count
+    for g in range(groups + 4):
+        for stage in range(5):
+            at = g - stage
+            if not 0 <= at < groups:
+                continue
+            if stage == 2:
+                compute(at * count, count)
+                continue
+            for step in range(at * count, at * count + count):
+                (forward, relay, None, exchange, finish)[stage](step)
     for copy in final:
         copy.wait()
 
@@ -293,6 +346,10 @@
 
 def vmem_specs(count):
     return [pl.BlockSpec(memory_space=pltpu.VMEM)] * count
+
+
+def hbm_specs(count):
+    return [pl.BlockSpec(memory_space=pltpu.HBM)] * count
 
 
 def params(number):
@@ -316,9 +373,15 @@
             jax.ShapeDtypeStruct(block, half),
             jax.ShapeDtypeStruct((8, token_count), full),
         ),
-        in_specs=vmem_specs(6),
+        in_specs=hbm_specs(3) + vmem_specs(1) + hbm_specs(2),
         out_specs=tuple(vmem_specs(2)),
         scratch_shapes=[
+            pltpu.VMEM(heads, half),
+            pltpu.VMEM(heads, half),
+            pltpu.VMEM(heads, half),
+            pltpu.VMEM(out_weight.shape, half),
+            pltpu.VMEM(block, half),
+            dma(5),
             pltpu.VMEM(heads, half),
             pltpu.VMEM(heads, half),
             pltpu.VMEM(heads, half),
@@ -342,43 +405,37 @@
     )(queries.reshape(heads), keys.reshape(heads), values.reshape(heads), cache, out_weight, residual)
 
 
-def fast_dispatch(taken, sp_count, tp_count, model_width):
-    capacity = taken.shape[1]
+def fast_experts(taken, gate_weight, up_weight, down_weight, sp_count, tp_count):
+    piece = taken.shape
+    capacity = piece[1]
+    model_width, hidden_width = gate_weight.shape[1:]
     row_count = tp_count // core_pair
+    half = jnp.bfloat16
+    wide = (sp_count, capacity, model_width)
+    pairs = (row_count, sp_count)
     return pl.pallas_call(
-        functools.partial(dispatch_kernel, sp_count, tp_count),
-        out_shape=jax.ShapeDtypeStruct((sp_count, capacity, model_width), jnp.bfloat16),
-        in_specs=vmem_specs(1),
+        functools.partial(expert_kernel, sp_count, tp_count),
+        out_shape=jax.ShapeDtypeStruct(piece, half),
+        in_specs=vmem_specs(1) + hbm_specs(3),
         out_specs=vmem_specs(1)[0],
         scratch_shapes=[
-            dma(sp_count), dma(sp_count), dma(row_count, sp_count), dma(row_count, sp_count),
-            dma(row_count, sp_count), dma(row_count, sp_count),
-        ],
-        compiler_params=params(1),
-    )(taken)
-
-
-def fast_collect(down, sp_count, tp_count):
-    capacity, local_width = down.shape[1], down.shape[2] // tp_count
-    row_count = tp_count // core_pair
-    piece = (sp_count, capacity, local_width)
-    half = jnp.bfloat16
-    return pl.pallas_call(
-        functools.partial(collect_kernel, sp_count, tp_count),
-        out_shape=jax.ShapeDtypeStruct(piece, half),
-        in_specs=vmem_specs(1),
-        out_specs=vmem_specs(1)[0],
-        scratch_shapes=[
+            pltpu.VMEM(gate_weight.shape[1:], half),
+            pltpu.VMEM(up_weight.shape[1:], half),
+            pltpu.VMEM(down_weight.shape[1:], half),
+            pltpu.VMEM(wide, half),
+            pltpu.VMEM((2 * capacity, hidden_width), half),
+            pltpu.VMEM(wide, half),
             pltpu.VMEM((row_count,) + piece, half),
             pltpu.VMEM((row_count,) + piece, half),
             pltpu.VMEM((row_count,) + piece, half),
             pltpu.VMEM(piece, half),
-            dma(row_count, sp_count), dma(row_count, sp_count),
-            dma(row_count, sp_count), dma(row_count, sp_count),
+            dma(3), dma(sp_count), dma(sp_count),
+            dma(*pairs), dma(*pairs), dma(*pairs), dma(*pairs),
+            dma(*pairs), dma(*pairs), dma(*pairs), dma(*pairs),
             dma(sp_count), dma(sp_count),
         ],
-        compiler_params=params(2),
-    )(down)
+        compiler_params=params(1),
+    )(taken, gate_weight, up_weight, down_weight)
 
 
 def ring_attention(
@@ -521,9 +578,10 @@
         .astype(jnp.bfloat16)
         .reshape(sp_count, capacity, local_width)
     )
-    direct = paired and capacity % 16 == 0
-    if direct:
-        arrived = fast_dispatch(taken_rows, sp_count, tp_count, model_width)
+    if paired and capacity % 16 == 0:
+        expert_back = fast_experts(
+            taken_rows, gate_weight, up_weight, down_weight, sp_count, tp_count
+        )
     else:
         arrived = lax.all_gather(
             lax.all_to_all(taken_rows, "sp", split_axis=0, concat_axis=0, tiled=True),
@@ -531,19 +589,17 @@
             axis=2,
             tiled=True,
         )
-    flat_rows = arrived.reshape(slot_total, model_width)
-    gate_value = jnp.dot(flat_rows, gate_weight[0], preferred_element_type=jnp.float32)
-    up_value = jnp.dot(flat_rows, up_weight[0], preferred_element_type=jnp.float32)
-    hidden = (jax.nn.silu(gate_value) * up_value).astype(jnp.bfloat16)
-    down_value = (
-        jnp.dot(hidden, down_weight[0], preferred_element_type=jnp.float32)
-        .astype(jnp.bfloat16)
-        .reshape(sp_count, capacity, model_width)
-    )
-    if direct:
-        expert_back = fast_collect(down_value, sp_count, tp_count)
-    else:
-        summed = lax.psum_scatter(down_value, "tp", scatter_dimension=2, tiled=True)
+        flat_rows = arrived.reshape(slot_total, model_width)
+        gate_value = jnp.dot(flat_rows, gate_weight[0], preferred_element_type=jnp.float32)
+        up_value = jnp.dot(flat_rows, up_weight[0], preferred_element_type=jnp.float32)
+        hidden = (jax.nn.silu(gate_value) * up_value).astype(jnp.bfloat16)
+        down_value = jnp.dot(hidden, down_weight[0], preferred_element_type=jnp.float32)
+        summed = lax.psum_scatter(
+            down_value.reshape(sp_count, capacity, model_width).astype(jnp.bfloat16),
+            "tp",
+            scatter_dimension=2,
+            tiled=True,
+        )
         expert_back = lax.all_to_all(summed, "sp", split_axis=0, concat_axis=0, tiled=True)
     back_rows = expert_back.reshape(slot_total, local_width)
     share = jnp.sum(

time: 135 us -> 120 us (0.89)
  matrix products: 17.8 us -> 1.88 us
  Pallas kernels: 104 us -> 107 us
  local copies, waits for them, and re-layouts: 10.1 us -> 8.38 us
    dot_general x2 -> x0, matrix products: 16 us -> none  [the longest x1 11.6 us: shards(): jnp.dot(hidden, down_weight[0], preferred_element_type=jnp.float32)]
    pallas_call x2 -> x1, Pallas kernels: 52.5 us -> 55.7 us  [fast_experts(): pl.pallas_call(functools.partial(expert_kernel, sp_count, tp_count), out_...]
    unnamed x17 -> x13, local copies, waits for them, and re-layouts: 7.95 us -> 6.2 us
where the time goes in v2:
time: 120 us
  Pallas kernels  107 us (89%)
  local copies, waits for them, and re-layouts  8.38 us (7%)
  other arithmetic  2.41 us (2%)
  matrix products  1.88 us (2%)
    pallas_call x1, Pallas kernels, fast_experts(): pl.pallas_call(functools.partial(expert_kernel, sp_count, tp_count), out_...  55.7 us
    pallas_call x1, Pallas kernels, fast_attention(): pl.pallas_call(functools.partial(attend_kernel, sp_count, tp_count), out_...  51.5 us
    unnamed x13, local copies, waits for them, and re-layouts  6.2 us

profile of v2, /device:TPU:0, one launch (start us, length us, event | category | flops | bytes accessed | tf_op | source)
XLA Modules:
  0.0 120.0 jit_solution(7717988129076890653)
XLA Ops:
  0.0 0.8 dynamic_slice.3
  0.8 0.7 broadcast_in_dim.10.c_ref
  1.5 0.8 copy.27
  2.3 0.1 eq.55
  2.4 0.1 eq.51
  2.6 1.1 reduce-window.6
  3.7 0.2 slice_reduce_fusion
  4.0 0.1 fusion.12
  4.1 0.1 reduce_sum.21
  4.2 0.1 copy.29
  4.3 0.7 multiply_add_fusion
  5.0 0.2 fusion
  5.2 0.0 copy-start
  5.2 1.6 %copy-done = bf16[512,2048]{1,0:T(8,128)(2,1)S(1)} copy-done((bf16[512,2048]{1,0:T(8,128)(2,1)S(1)}, bf16[512,2048]{1,0:T(8,128)(2,1)}, u32[]{:S(2)}) %copy-start) | copy-done | bytes 2097176
  6.8 0.9 copy-done.1
  7.8 0.9 copy-done.2
  8.7 0.9 copy-done.3
  9.7 0.9 copy-done.4
  10.6 51.5 %shard_map.118 = (bf16[256,512]{1,0:T(8,128)(2,1)S(1)}, f32[8,256]{1,0:T(8,128)S(1)}) custom-call(bf16[8,64,256]{2,1,0:T(8,128)(2,1)S(1)} %bitcast.21, bf16[8,64,256]{2,1,0:T(8,128)(2,1)S(1)} %bitcast.22, bf16[8,64,256]{2,1,0:T(8,128)(2,1)S(1)} %bitcast.23, f32[8,8,256]{2,1,0:T(8,128)S(1)} %broadcast_in_dim.10.c_ref, bf16[512,2048]{1,0:T(8,128)(2,1)S(1)} %copy-done, ...), custom_call_target="tpu_custom_call" | custom-call | tf_op jit(solution)/shard_map/pallas_call | solution.py:370
  62.1 0.4 convolution_convert_fusion
  62.6 55.7 %shard_map.119 = bf16[8,80,512]{2,1,0:T(8,128)(2,1)S(1)} custom-call(bf16[8,80,512]{2,1,0:T(8,128)(2,1)S(1)} %bitcast.20, bf16[1,2048,1024]{2,1,0:T(8,128)(2,1)} %g_hbm.1, bf16[1,2048,1024]{2,1,0:T(8,128)(2,1)} %u_hbm.1, bf16[1,1024,2048]{2,1,0:T(8,128)(2,1)} %d_hbm.1), custom_call_target="tpu_custom_call" | custom-call | tf_op jit(solution)/shard_map/pallas_call | solution.py:416
  118.3 0.2 select_reduce_fusion
  118.5 0.4 fusion.9
  118.9 1.1 fusion.2
  (10 shorter events, 0.1 us)
Async XLA Ops:
  5.2 1.6 %copy-start = (bf16[512,2048]{1,0:T(8,128)(2,1)S(1)}, bf16[512,2048]{1,0:T(8,128)(2,1)}, u32[]{:S(2)}) copy-start(bf16[512,2048]{1,0:T(8,128)(2,1)} %w_hbm.1) | copy-start | bytes 6291460
  6.8 0.9 copy-start.1
  7.8 0.9 copy-start.2
  8.7 0.9 copy-start.3
  9.7 0.9 copy-start.4
  62.6 55.7 %copy-start.5 = (f32[256,2]{0,1:T(2,128)S(1)}, f32[256,2]{0,1:T(2,128)}, u32[]{:S(2)}) copy-start(f32[256,2]{0,1:T(2,128)} %param.20) | copy-start | bytes 6148
